TPU v7x, 32 devices: a whole 2x2x4 slice. The times are simulated.
32 devices in a mesh: dp: 2 (over x), kv: 8 (over z, y), tp: 2 (over core).
Axes of the slice: x: 2, y: 2, z: 4, core: 2. Of those that a mesh axis runs over, the one named last changes fastest.
Arguments:
- tokens: bfloat16 [32, 16, 2048], P('dp', None, ('kv', 'tp')), may hold values from -190 to 190
- gain_in: float32 [2048], P(('kv', 'tp')), may hold values from 0.1 to 1.9
- w_qdown: bfloat16 [2048, 512], P(('kv', 'tp')), may hold values from -0.125 to 0.125
- w_kvdown: bfloat16 [2048, 256], P(('kv', 'tp')), may hold values from -0.125 to 0.125
- w_ropek: bfloat16 [2048, 32], replicated, may hold values from -0.125 to 0.125
- gain_qlat: float32 [512], replicated, may hold values from 0.1 to 1.9
- gain_kvlat: float32 [256], replicated, may hold values from 0.1 to 1.9
- w_qup: bfloat16 [512, 16, 96], P(None, 'tp'), may hold values from -0.25 to 0.25
- gain_q: float32 [96], replicated, may hold values from 0.4 to 20
- w_ukey: bfloat16 [256, 16, 64], P(None, 'tp'), may hold values from -0.75 to 0.75
- w_uval: bfloat16 [256, 16, 128], P(None, 'tp'), may hold values from -0.375 to 0.375
- w_out: bfloat16 [2048, 2048], P('tp', 'kv'), may hold values from -2.5 to 2.5
- gain_out: float32 [2048], P(('kv', 'tp')), may hold values from 0.1 to 1.9
- cache_lat: bfloat16 [32, 2048, 256], P('dp', 'kv'), may hold values from -6 to 6
- cache_rope: bfloat16 [32, 32, 2048], P('dp', None, 'kv'), may hold values from -6 to 6
- parents: int32 [32, 16], P('dp'), may hold values from -1 to 14, as said below
- lengths: int32 [32], P('dp'), may hold values from 1024 to 2016
- accepted: int32 [32], P('dp'), may hold values from 0 to 16
Outputs:
- attn_out: bfloat16 [32, 16, 2048], P('dp', None, ('kv', 'tp'))
- lat_cache_out: bfloat16 [32, 2048, 256], P('dp', 'kv')
- rope_cache_out: bfloat16 [32, 32, 2048], P('dp', None, 'kv')
Inputs may be any that keep to these rules, and one draw needn't show every extreme that they name: `parents`: proposal j's parent is -1 (the last accepted token) or a proposal before j. Rows 0 .. lengths + accepted - 1 of a sequence's cache hold its past; the 16 positions after them lie inside the cache.
All inputs are finite; a program needn't handle non-finite values.
Results may differ from a plain program's by a relative error of at most 0.0102.
The roundings to bfloat16 on the way count: a program that leaves them out, or rounds other values in their place, can miss the bound.
Values may be sent and summed in bfloat16 or wider, within the bound.
A program may use at most 64 MiB of HBM per device.

v0:
```python
import jax
import jax.numpy as jnp
from jax import lax
from jax.sharding import PartitionSpec as P

epsilon = 1e-06


def normed(values, gain_vec):
    return (
        values * lax.rsqrt(jnp.mean(values * values, axis=-1, keepdims=True) + epsilon) * gain_vec
    )


def rope_angles(position, half_dim):
    frequency = 10000.0 ** (-(jnp.arange(half_dim, dtype=jnp.float32) * 2.0) / (2 * half_dim))
    return position.astype(jnp.float32)[..., None] * frequency


def ancestry(parents):
    proposals = parents.shape[-1]
    parent_link = (parents[..., :, None] == jnp.arange(proposals, dtype=jnp.int32)).astype(
        jnp.float32
    )
    identity = jnp.broadcast_to(jnp.eye(proposals, dtype=jnp.float32), parent_link.shape)

    def extend(iteration, state_pair):
        reaches, current = state_pair
        current = jnp.einsum("sij,sjk->sik", current, parent_link, precision=lax.Precision.HIGHEST)
        return (reaches + current, current)

    reaches, current = lax.fori_loop(0, proposals - 1, extend, (identity, identity))
    depths = (jnp.sum(reaches, axis=-1) - 1.0).astype(jnp.int32)
    return (reaches, depths)


def latents(summed, squares, full_width, gain_qlat, gain_kvlat):
    qrank = gain_qlat.shape[0]
    kvrank = gain_kvlat.shape[0]
    scaled_rows = summed * lax.rsqrt(squares / full_width + epsilon)[:, None]
    query_latent = normed(scaled_rows[:, :qrank], gain_qlat).astype(jnp.bfloat16)
    new_latent = normed(scaled_rows[:, qrank : qrank + kvrank], gain_kvlat).astype(jnp.bfloat16)
    new_rope = scaled_rows[:, qrank + kvrank :].astype(jnp.bfloat16)
    return (query_latent, new_latent, new_rope)


def apply_values(numer_rows, value_map):
    return jnp.einsum("...hk,khv->...hv", numer_rows, value_map, precision=lax.Precision.HIGHEST)


def local(
    tokens,
    gain_in,
    w_qdown,
    w_kvdown,
    w_ropek,
    gain_qlat,
    gain_kvlat,
    w_qup,
    gain_q,
    w_ukey,
    w_uval,
    w_out,
    gain_out,
    cache_lat,
    cache_rope,
    parents,
    lengths,
    accepted,
):
    seq_count, proposals, local_width = tokens.shape
    full_width = local_width * lax.axis_size(("kv", "tp"))
    tok_rows = tokens.astype(jnp.float32).reshape(seq_count * proposals, local_width)
    scaled = (tok_rows * gain_in).astype(jnp.bfloat16)
    squares = jnp.sum(tok_rows * tok_rows, axis=-1)
    rope_rows = lax.dynamic_slice_in_dim(
        w_ropek, lax.axis_index(("kv", "tp")) * local_width, local_width, 0
    )
    joined = jnp.concatenate([w_qdown, w_kvdown, rope_rows], axis=1)
    partial_rows = jnp.dot(scaled, joined, preferred_element_type=jnp.float32)
    summed, total_squares = lax.psum((partial_rows, squares), ("kv", "tp"))
    query_latent, new_latent, new_rope = latents(
        summed, total_squares, full_width, gain_qlat, gain_kvlat
    )
    qrank = w_qup.shape[0]
    heads_here = w_qup.shape[1]
    qkhead = w_qup.shape[2]
    kvrank = w_ukey.shape[0]
    nope_dim = w_ukey.shape[2]
    vhead = w_uval.shape[2]
    rope_dim = cache_rope.shape[1]
    half_dim = rope_dim // 2
    reaches, depths = ancestry(parents)
    starts = lengths + accepted
    query_pos = starts[:, None] + depths
    queries = jnp.dot(
        query_latent, w_qup.reshape(qrank, heads_here * qkhead), preferred_element_type=jnp.float32
    )
    queries = normed(queries.reshape(seq_count, proposals, heads_here, qkhead), gain_q)
    query_nope = queries[..., :nope_dim].astype(jnp.bfloat16)
    angles = rope_angles(query_pos, half_dim)[:, :, None, :]
    cosine = jnp.cos(angles)
    sines = jnp.sin(angles)
    lower_half = queries[..., nope_dim : nope_dim + half_dim]
    upper_half = queries[..., nope_dim + half_dim :]
    query_rot = jnp.concatenate(
        [lower_half * cosine - upper_half * sines, upper_half * cosine + lower_half * sines],
        axis=-1,
    ).astype(jnp.bfloat16)
    query_lat = jnp.einsum(
        "sihn,khn->sihk", query_nope, w_ukey, preferred_element_type=jnp.float32
    ).astype(jnp.bfloat16)
    pos_count = cache_lat.shape[1]
    slots = lax.axis_index("kv") * pos_count + jnp.arange(pos_count, dtype=jnp.int32)
    offset = slots[None, :] - starts[:, None]
    inside = (offset >= 0) & (offset < proposals)
    matches = offset[:, :, None] == jnp.arange(proposals, dtype=jnp.int32)
    selector = matches.astype(jnp.bfloat16)
    new_latent = new_latent.reshape(seq_count, proposals, kvrank)
    new_rope = new_rope.reshape(seq_count, proposals, rope_dim)
    placed = jnp.einsum(
        "spj,sjk->spk", selector, new_latent, preferred_element_type=jnp.float32
    ).astype(jnp.bfloat16)
    lat_out = jnp.where(inside[:, :, None], placed, cache_lat)
    placed_rope = jnp.einsum(
        "spj,sjr->srp", selector, new_rope, preferred_element_type=jnp.float32
    ).astype(jnp.bfloat16)
    rope_out = jnp.where(inside[:, None, :], placed_rope, cache_rope)
    key_pos = jnp.where(
        inside,
        starts[:, None] + jnp.sum(jnp.where(matches, depths[:, None, :], 0), axis=-1),
        slots[None, :],
    )
    ancestor = jnp.einsum(
        "sij,spj->sip", reaches, matches.astype(jnp.float32), precision=lax.Precision.HIGHEST
    )
    visible = (offset < 0)[:, None, :] | (ancestor > 0.5)
    key_angles = jnp.swapaxes(rope_angles(key_pos, half_dim), 1, 2)
    key_cos = jnp.cos(key_angles)
    key_sin = jnp.sin(key_angles)
    rope32 = rope_out.astype(jnp.float32)
    key_low = rope32[:, :half_dim, :]
    key_high = rope32[:, half_dim:, :]
    key_rot = jnp.concatenate(
        [key_low * key_cos - key_high * key_sin, key_high * key_cos + key_low * key_sin], axis=1
    ).astype(jnp.bfloat16)
    scores = (
        jnp.einsum("sihk,spk->sihp", query_lat, lat_out, preferred_element_type=jnp.float32)
        + jnp.einsum("sihr,srp->sihp", query_rot, key_rot, preferred_element_type=jnp.float32)
    ) * qkhead ** (-0.5)
    masked = jnp.where(visible[:, :, None, :], scores, -jnp.inf)
    row_max = lax.pmax(jnp.max(masked, axis=-1), "kv")
    weights32 = jnp.exp(masked - row_max[..., None])
    denominator = jnp.sum(weights32, axis=-1)
    weights = weights32.astype(jnp.bfloat16)
    numerator = jnp.einsum("sihp,spk->sihk", weights, lat_out, preferred_element_type=jnp.float32)
    value_map = w_uval.astype(jnp.float32)
    numer_values = apply_values(numerator, value_map)
    values_all, denom_all = lax.psum((numer_values, denominator), "kv")
    head_out = (values_all / denom_all[..., None]).astype(jnp.bfloat16)
    head_rows = head_out.reshape(seq_count * proposals, heads_here * vhead)
    partial_out = jnp.dot(head_rows, w_out, preferred_element_type=jnp.float32).reshape(
        seq_count, proposals, w_out.shape[1]
    )
    mixed = lax.psum_scatter(partial_out, "tp", scatter_dimension=2, tiled=True)
    local_squares = jnp.sum(mixed * mixed, axis=-1)
    norm_total = lax.psum(local_squares, ("kv", "tp"))
    result = (mixed * lax.rsqrt(norm_total / full_width + epsilon)[..., None] * gain_out).astype(
        jnp.bfloat16
    )
    return (result, lat_out, rope_out)


def solution(mesh):
    placed = (
        P("dp", None, ("kv", "tp")),
        P(("kv", "tp")),
        P(("kv", "tp"), None),
        P(("kv", "tp"), None),
        P(),
        P(),
        P(),
        P(None, "tp", None),
        P(),
        P(None, "tp", None),
        P(None, "tp", None),
        P("tp", "kv"),
        P(("kv", "tp")),
        P("dp", "kv", None),
        P("dp", None, "kv"),
        P("dp", None),
        P("dp"),
        P("dp"),
    )
    return jax.shard_map(
        local,
        mesh=mesh,
        in_specs=placed,
        out_specs=(P("dp", None, ("kv", "tp")), P("dp", "kv", None), P("dp", None, "kv")),
        check_vma=False,
    )
```

profile of v0, /device:TPU:0, one launch (start us, length us, event | category | flops | bytes accessed | tf_op | source)
XLA Modules:
  0.0 292.3 jit_solution(4244914604734968146)
XLA Ops:
  7.3 0.8 constant_dynamic-slice_fusion
  8.2 0.9 fusion.43
  9.0 2.2 fusion.37
  11.7 5.6 %while.13 = (s32[]{:T(128)}, f32[16,16,16]{2,1,0:T(8,128)S(1)}, f32[16,16,16]{2,1,0:T(8,128)S(1)}, s32[16,16]{1,0:T(8,128)S(1)}, s32[]{:T(128)}) while((s32[]{:T(128)}, f32[16,16,16]{2,1,0:T(8,128)S(1)}, f32[16,16,16]{2,1,0:T(8,128)S(1)}, s32[16,16]{1,0:T(8,128)S(1)}, s32[]{:T(128)}) %tuple.45), condition=%wide.region_1.0_spmd.clone, body=%wide.region_0.0_spmd.clone.sunk | while | flops 798722 | bytes 99389 | solution.py:32
  11.7 0.3 fusion.67
  12.1 0.3 fusion.67
  17.6 35.1 %psum.36 = f32[256]{0:T(256)S(1)} all-reduce(f32[256]{0:T(256)S(1)} %reduce_sum.75), channel_id=1, replica_groups=mesh['dp'=2,'kv'=8,'tp'=2] {'kv','tp'}, use_global_device_ids=true, to_apply=%region_4.0 | all-reduce | flops 256 | bytes 2048 | tf_op jit(solution)/shard_map/psum | solution.py:81
  53.2 0.5 multiply_cosine_fusion.1
  53.7 53.2 %all-reduce.3.cloned.1.call-done = f32[256,800]{0,1:T(8,128)} async-done(((f32[256,800]{0,1:T(8,128)}), f32[256,800]{0,1:T(8,128)}) %all-reduce.3.cloned.1.call-update) | async-done | bytes 819216 | tf_op jit(solution)/shard_map/psum | solution.py:81
  107.0 1.2 broadcast_multiply_fusion
  109.0 0.6 multiply_reduce_fusion
  109.7 1.0 fusion.52
  110.7 1.1 fusion.31
  111.8 0.3 multiply_multiply_fusion
  112.2 0.4 fusion.11
  112.6 0.6 subtract_convert_fusion
  113.5 0.7 copy-done.2
  114.2 1.4 convert_select_fusion
  115.6 0.9 fusion.5
  116.5 2.0 fusion.53
  118.5 37.9 %pmax.7 = f32[16,16,8]{2,1,0:T(8,128)S(1)} all-reduce(f32[16,16,8]{2,1,0:T(8,128)S(1)} %get-tuple-element.61), channel_id=1, replica_groups=mesh['dp'=2,'kv'=8,'tp'=2] {'kv'}, use_global_device_ids=true, to_apply=%region_11.12 | all-reduce | flops 2048 | bytes 16384 | tf_op jit(solution)/shard_map/pmax | solution.py:152
  156.4 2.3 fusion.9
  158.7 0.5 fusion.7
  159.2 0.6 copy-done.3
  159.7 2.1 convolution_bitcast_fusion
  161.9 35.7 %psum.38 = f32[16,16,8]{2,1,0:T(8,128)S(1)} all-reduce(f32[16,16,8]{2,1,0:T(8,128)S(1)} %get-tuple-element.47), channel_id=1, replica_groups=mesh['dp'=2,'kv'=8,'tp'=2] {'kv'}, use_global_device_ids=true, to_apply=%region_14.15 | all-reduce | flops 2048 | bytes 16384 | tf_op jit(solution)/shard_map/psum | solution.py:159
  197.8 41.0 %all-reduce.5.cloned.1.call-done = f32[16,16,8,128]{3,1,0,2:T(8,128)} async-done(((f32[16,16,8,128]{3,1,0,2:T(8,128)}), f32[16,16,8,128]{3,1,0,2:T(8,128)}) %all-reduce.5.cloned.1.call-update) | async-done | bytes 1048592 | tf_op jit(solution)/shard_map/psum | solution.py:159
  238.8 2.4 fusion.18
  241.2 7.5 %reduce-scatter.2.cloned.1.call-done = f32[16,16,128]{2,1,0:T(8,128)} async-done(((f32[16,16,256]{2,1,0:T(8,128)}), f32[16,16,128]{2,1,0:T(8,128)}) %reduce-scatter.2.cloned.1.call-update) | async-done | bytes 131088 | tf_op jit(solution)/shard_map/reduce_scatter | solution.py:165
  248.7 1.0 multiply_reduce_fusion.3
  249.7 34.4 %psum.39 = f32[16,16]{1,0:T(8,128)S(1)} all-reduce(f32[16,16]{1,0:T(8,128)S(1)} %multiply_reduce_fusion.3), channel_id=1, replica_groups=mesh['dp'=2,'kv'=8,'tp'=2] {'kv','tp'}, use_global_device_ids=true, to_apply=%region_17.18 | all-reduce | flops 256 | bytes 2048 | tf_op jit(solution)/shard_map/psum | solution.py:167
  284.1 1.6 multiply_convert_fusion.2
  (94 shorter events, 7.1 us)
Async XLA Ops:
  7.2 101.8 %copy-start = (bf16[512,8,96]{0,2,1:T(8,128)(2,1)S(1)}, bf16[512,8,96]{0,2,1:T(8,128)(2,1)}, u32[]{:S(2)}) copy-start(bf16[512,8,96]{0,2,1:T(8,128)(2,1)} %param.27) | copy-start | bytes 2359300
  7.2 4.1 %copy-start.6 = (bf16[16,16,128]{2,1,0:T(8,128)(2,1)S(1)}, bf16[16,16,128]{2,1,0:T(8,128)(2,1)}, u32[]{:S(2)}) copy-start(bf16[16,16,128]{2,1,0:T(8,128)(2,1)} %param.20) | copy-start | bytes 196612
  7.2 4.2 %copy-start.14 = (s32[16]{0:T(128)S(1)}, s32[16]{0:T(128)}, u32[]{:S(2)}) copy-start(s32[16]{0:T(128)} %param.37) | copy-start | bytes 196
  7.2 4.2 %copy-start.13 = (s32[16]{0:T(128)S(1)}, s32[16]{0:T(128)}, u32[]{:S(2)}) copy-start(s32[16]{0:T(128)} %param.36) | copy-start | bytes 196
  7.2 4.4 %copy-start.7 = (s32[16,16]{1,0:T(8,128)S(1)}, s32[16,16]{1,0:T(8,128)}, u32[]{:S(2)}) copy-start(s32[16,16]{1,0:T(8,128)} %param.35) | copy-start | bytes 3076
  7.2 99.7 %all-reduce.3.cloned.1.call-start = ((), (), s32[]{:S(2)}) async-start(), calls=%async_computation.1 | async-start | bytes 1638400 | tf_op jit(solution)/shard_map/psum | solution.py:81
  11.2 227.5 %all-reduce.5.cloned.1.call-start = ((), (), s32[]{:S(2)}) async-start(), calls=%async_computation.2 | async-start | bytes 2097152 | tf_op jit(solution)/shard_map/psum | solution.py:159
  17.3 91.2 %copy-start.8 = (f32[512]{0:T(512)S(1)}, f32[512]{0:T(512)}, u32[]{:S(2)}) copy-start(f32[512]{0:T(512)} %param.25) | copy-start | bytes 6148
  53.0 55.8 %copy-start.9 = (f32[256]{0:T(256)S(1)}, f32[256]{0:T(256)}, u32[]{:S(2)}) copy-start(f32[256]{0:T(256)} %param.26) | copy-start | bytes 3076
  108.5 1.2 copy-start.4
  109.0 2.8 copy-start.10
  109.6 2.5 copy-start.5
  112.6 1.6 copy-start.2
  115.6 43.1 %copy-start.1 = (bf16[16,256,256]{2,1,0:T(8,128)(2,1)}, bf16[16,256,256]{2,1,0:T(8,128)(2,1)S(1)}, u32[]{:S(2)}) copy-start(bf16[16,256,256]{2,1,0:T(8,128)(2,1)S(1)} %convert_select_fusion) | copy-start | bytes 6291460
  158.7 1.0 copy-start.3
  159.7 79.0 %copy-start.12 = (bf16[1024,256]{1,0:T(8,128)(2,1)S(1)}, bf16[1024,256]{1,0:T(8,128)(2,1)}, u32[]{:S(2)}) copy-start(bf16[1024,256]{1,0:T(8,128)(2,1)} %param.31) | copy-start | bytes 1572868
  161.9 86.8 %reduce-scatter.2.cloned.1.call-start = ((), (), s32[]{:S(2)}) async-start(), calls=%async_computation.3 | async-start | bytes 393216 | tf_op jit(solution)/shard_map/reduce_scatter | solution.py:165
  197.8 86.3 %copy-start.11 = (f32[128]{0:T(128)S(1)}, f32[128]{0:T(128)}, u32[]{:S(2)}) copy-start(f32[128]{0:T(128)} %param.32) | copy-start | bytes 1540
Sparse Core Ops, SparseCore 0:
  12.1 94.8 all-reduce.2
  162.0 76.7 all-reduce.4
  241.3 7.3 reduce-scatter.1
where the time goes:
time: 293 us; the launch traced here: 292 us
  blocking collectives  143 us (49%)
  waiting for transfers between devices  102 us (35%)
  matrix products  18.7 us (6%)
  between operations  14.2 us (5%)
  other arithmetic  11 us (4%)
    psum x1, waiting for transfers between devices, local(): summed, total_squares = lax.psum((partial_rows, squares), ('kv', 'tp'))  53.2 us
    psum x1, waiting for transfers between devices, local(): values_all, denom_all = lax.psum((numer_values, denominator), 'kv')  41 us
    pmax x1, blocking collectives, local(): row_max = lax.pmax(jnp.max(masked, axis=-1), 'kv')  37.9 us
    psum x1, blocking collectives, local(): values_all, denom_all = lax.psum((numer_values, denominator), 'kv')  35.7 us
    psum x1, blocking collectives, local(): summed, total_squares = lax.psum((partial_rows, squares), ('kv', 'tp'))  35.1 us
    psum x1, blocking collectives, local(): norm_total = lax.psum(local_squares, ('kv', 'tp'))  34.4 us
    reduce_scatter x1, waiting for transfers between devices, local(): mixed = lax.psum_scatter(partial_out, 'tp', scatter_dimension=2, tiled=True)  7.5 us
  transfers between devices with their start and end apart: 3, of which 3 were waited for; matrix products, arithmetic and copies ran while one was open for 2% of the time, Pallas kernels for 0%

commit v1 on v0

--- a/solution.py
+++ b/solution.py
@@ -164,7 +164,7 @@
     )
     mixed = lax.psum_scatter(partial_out, "tp", scatter_dimension=2, tiled=True)
     local_squares = jnp.sum(mixed * mixed, axis=-1)
-    norm_total = lax.psum(local_squares, ("kv", "tp"))
+    norm_total = jnp.sum(lax.all_gather(local_squares, ("kv", "tp")), axis=0)
     result = (mixed * lax.rsqrt(norm_total / full_width + epsilon)[..., None] * gain_out).astype(
         jnp.bfloat16
     )

time: 293 us -> 280 us (0.956)
  blocking collectives: 143 us -> 131 us
    psum x1 -> x0, blocking collectives: 34.4 us -> none  [local(): norm_total = lax.psum(local_squares, ('kv', 'tp'))]
    all_gather x0 -> x1, blocking collectives: none -> 21.9 us  [local(): norm_total = jnp.sum(lax.all_gather(local_squares, ('kv', 'tp')), axis=0)]
where the time goes in v1:
time: 280 us
  blocking collectives  131 us (47%)
  waiting for transfers between devices  102 us (36%)
  matrix products  18.7 us (7%)
  between operations  14.2 us (5%)
  other arithmetic  11 us (4%)
  local copies, waits for them, and re-layouts  2.92 us (1%)
    psum x1, waiting for transfers between devices, local(): summed, total_squares = lax.psum((partial_rows, squares), ('kv', 'tp'))  53.2 us
    psum x1, waiting for transfers between devices, local(): values_all, denom_all = lax.psum((numer_values, denominator), 'kv')  41 us
    pmax x1, blocking collectives, local(): row_max = lax.pmax(jnp.max(masked, axis=-1), 'kv')  37.9 us
    psum x1, blocking collectives, local(): values_all, denom_all = lax.psum((numer_values, denominator), 'kv')  35.7 us
    psum x1, blocking collectives, local(): summed, total_squares = lax.psum((partial_rows, squares), ('kv', 'tp'))  35.1 us
    all_gather x1, blocking collectives, local(): norm_total = jnp.sum(lax.all_gather(local_squares, ('kv', 'tp')), axis=0)  21.9 us
    reduce_scatter x1, waiting for transfers between devices, local(): mixed = lax.psum_scatter(partial_out, 'tp', scatter_dimension=2, tiled=True)  7.5 us
  transfers between devices with their start and end apart: 3, of which 3 were waited for; matrix products, arithmetic and copies ran while one was open for 2% of the time, Pallas kernels for 0%

profile of v1, /device:TPU:0, one launch (start us, length us, event | category | flops | bytes accessed | tf_op | source)
XLA Modules:
  0.0 279.8 jit_solution(1081908613193791656)
XLA Ops:
  7.3 0.8 constant_dynamic-slice_fusion
  8.2 0.9 fusion.43
  9.0 2.2 fusion.37
  11.7 5.6 %while.13 = (s32[]{:T(128)}, f32[16,16,16]{2,1,0:T(8,128)S(1)}, f32[16,16,16]{2,1,0:T(8,128)S(1)}, s32[16,16]{1,0:T(8,128)S(1)}, s32[]{:T(128)}) while((s32[]{:T(128)}, f32[16,16,16]{2,1,0:T(8,128)S(1)}, f32[16,16,16]{2,1,0:T(8,128)S(1)}, s32[16,16]{1,0:T(8,128)S(1)}, s32[]{:T(128)}) %tuple.45), condition=%wide.region_1.0_spmd.clone, body=%wide.region_0.0_spmd.clone.sunk | while | flops 798722 | bytes 99389 | solution.py:32
  11.7 0.3 fusion.67
  12.1 0.3 fusion.67
  17.6 35.1 %psum.29 = f32[256]{0:T(256)S(1)} all-reduce(f32[256]{0:T(256)S(1)} %reduce_sum.84), channel_id=1, replica_groups=mesh['dp'=2,'kv'=8,'tp'=2] {'kv','tp'}, use_global_device_ids=true, to_apply=%region_4.0 | all-reduce | flops 256 | bytes 2048 | tf_op jit(solution)/shard_map/psum | solution.py:81
  53.2 0.5 multiply_cosine_fusion.1
  53.7 53.2 %all-reduce.3.cloned.1.call-done = f32[256,800]{0,1:T(8,128)} async-done(((f32[256,800]{0,1:T(8,128)}), f32[256,800]{0,1:T(8,128)}) %all-reduce.3.cloned.1.call-update) | async-done | bytes 819216 | tf_op jit(solution)/shard_map/psum | solution.py:81
  107.0 1.2 broadcast_multiply_fusion
  109.0 0.6 multiply_reduce_fusion
  109.7 1.0 fusion.52
  110.7 1.1 fusion.31
  111.8 0.3 multiply_multiply_fusion
  112.2 0.4 fusion.11
  112.6 0.6 subtract_convert_fusion
  113.5 0.7 copy-done.2
  114.2 1.4 convert_select_fusion
  115.6 0.9 fusion.5
  116.5 2.0 fusion.53
  118.5 37.9 %pmax.7 = f32[16,16,8]{2,1,0:T(8,128)S(1)} all-reduce(f32[16,16,8]{2,1,0:T(8,128)S(1)} %get-tuple-element.61), channel_id=1, replica_groups=mesh['dp'=2,'kv'=8,'tp'=2] {'kv'}, use_global_device_ids=true, to_apply=%region_11.12 | all-reduce | flops 2048 | bytes 16384 | tf_op jit(solution)/shard_map/pmax | solution.py:152
  156.4 2.3 fusion.9
  158.7 0.5 fusion.7
  159.2 0.6 copy-done.3
  159.7 2.1 convolution_bitcast_fusion
  161.9 35.7 %psum.31 = f32[16,16,8]{2,1,0:T(8,128)S(1)} all-reduce(f32[16,16,8]{2,1,0:T(8,128)S(1)} %get-tuple-element.47), channel_id=1, replica_groups=mesh['dp'=2,'kv'=8,'tp'=2] {'kv'}, use_global_device_ids=true, to_apply=%region_14.15 | all-reduce | flops 2048 | bytes 16384 | tf_op jit(solution)/shard_map/psum | solution.py:159
  197.8 41.0 %all-reduce.5.cloned.1.call-done = f32[16,16,8,128]{3,1,0,2:T(8,128)} async-done(((f32[16,16,8,128]{3,1,0,2:T(8,128)}), f32[16,16,8,128]{3,1,0,2:T(8,128)}) %all-reduce.5.cloned.1.call-update) | async-done | bytes 1048592 | tf_op jit(solution)/shard_map/psum | solution.py:159
  238.8 2.4 fusion.18
  241.2 7.5 %reduce-scatter.2.cloned.1.call-done = f32[16,16,128]{2,1,0:T(8,128)} async-done(((f32[16,16,256]{2,1,0:T(8,128)}), f32[16,16,128]{2,1,0:T(8,128)}) %reduce-scatter.2.cloned.1.call-update) | async-done | bytes 131088 | tf_op jit(solution)/shard_map/reduce_scatter | solution.py:165
  248.7 1.0 multiply_reduce_fusion.3
  249.7 21.9 %all-gather = f32[256,16]{1,0:T(8,128)S(1)} all-gather(f32[16,16]{1,0:T(8,128)S(1)} %multiply_reduce_fusion.3), channel_id=2, replica_groups=mesh['dp'=2,'kv'=8,'tp'=2] {'kv','tp'}, dimensions={0}, use_global_device_ids=true | all-gather | bytes 17408 | tf_op jit(solution)/shard_map/all_gather | solution.py:167
  271.6 1.6 multiply_convert_fusion.2
  (95 shorter events, 7.1 us)
Async XLA Ops:
  7.2 101.8 %copy-start = (bf16[512,8,96]{0,2,1:T(8,128)(2,1)S(1)}, bf16[512,8,96]{0,2,1:T(8,128)(2,1)}, u32[]{:S(2)}) copy-start(bf16[512,8,96]{0,2,1:T(8,128)(2,1)} %param.27) | copy-start | bytes 2359300
  7.2 4.1 %copy-start.6 = (bf16[16,16,128]{2,1,0:T(8,128)(2,1)S(1)}, bf16[16,16,128]{2,1,0:T(8,128)(2,1)}, u32[]{:S(2)}) copy-start(bf16[16,16,128]{2,1,0:T(8,128)(2,1)} %param.20) | copy-start | bytes 196612
  7.2 4.2 %copy-start.14 = (s32[16]{0:T(128)S(1)}, s32[16]{0:T(128)}, u32[]{:S(2)}) copy-start(s32[16]{0:T(128)} %param.37) | copy-start | bytes 196
  7.2 4.2 %copy-start.13 = (s32[16]{0:T(128)S(1)}, s32[16]{0:T(128)}, u32[]{:S(2)}) copy-start(s32[16]{0:T(128)} %param.36) | copy-start | bytes 196
  7.2 4.4 %copy-start.7 = (s32[16,16]{1,0:T(8,128)S(1)}, s32[16,16]{1,0:T(8,128)}, u32[]{:S(2)}) copy-start(s32[16,16]{1,0:T(8,128)} %param.35) | copy-start | bytes 3076
  7.2 99.7 %all-reduce.3.cloned.1.call-start = ((), (), s32[]{:S(2)}) async-start(), calls=%async_computation.1 | async-start | bytes 1638400 | tf_op jit(solution)/shard_map/psum | solution.py:81
  11.2 227.5 %all-reduce.5.cloned.1.call-start = ((), (), s32[]{:S(2)}) async-start(), calls=%async_computation.2 | async-start | bytes 2097152 | tf_op jit(solution)/shard_map/psum | solution.py:159
  17.3 91.2 %copy-start.8 = (f32[512]{0:T(512)S(1)}, f32[512]{0:T(512)}, u32[]{:S(2)}) copy-start(f32[512]{0:T(512)} %param.25) | copy-start | bytes 6148
  53.0 55.8 %copy-start.9 = (f32[256]{0:T(256)S(1)}, f32[256]{0:T(256)}, u32[]{:S(2)}) copy-start(f32[256]{0:T(256)} %param.26) | copy-start | bytes 3076
  108.5 1.2 copy-start.4
  109.0 2.8 %copy-start.10 = (f32[96]{0:T(128)S(1)}, f32[96]{0:T(128)}, u32[]{:S(2)}) copy-start(f32[96]{0:T(128)} %param.28) | copy-start | bytes 1156
  109.6 2.5 copy-start.5
  112.6 1.6 copy-start.2
  115.6 43.1 %copy-start.1 = (bf16[16,256,256]{2,1,0:T(8,128)(2,1)}, bf16[16,256,256]{2,1,0:T(8,128)(2,1)S(1)}, u32[]{:S(2)}) copy-start(bf16[16,256,256]{2,1,0:T(8,128)(2,1)S(1)} %convert_select_fusion) | copy-start | bytes 6291460
  158.7 1.0 copy-start.3
  159.7 79.0 %copy-start.12 = (bf16[1024,256]{1,0:T(8,128)(2,1)S(1)}, bf16[1024,256]{1,0:T(8,128)(2,1)}, u32[]{:S(2)}) copy-start(bf16[1024,256]{1,0:T(8,128)(2,1)} %param.31) | copy-start | bytes 1572868
  161.9 86.8 %reduce-scatter.2.cloned.1.call-start = ((), (), s32[]{:S(2)}) async-start(), calls=%async_computation.3 | async-start | bytes 393216 | tf_op jit(solution)/shard_map/reduce_scatter | solution.py:165
  197.8 73.9 %copy-start.11 = (f32[128]{0:T(128)S(1)}, f32[128]{0:T(128)}, u32[]{:S(2)}) copy-start(f32[128]{0:T(128)} %param.32) | copy-start | bytes 1540
Sparse Core Ops, SparseCore 0:
  12.1 94.8 all-reduce.2
  162.0 76.7 all-reduce.4
  241.3 7.3 reduce-scatter.1
